TPU v7x, 512 devices: a whole 4x8x8 slice. The times are simulated.
512 devices in a mesh: sp: 32 (over z, x), tp: 16 (over y, core).
Axes of the slice: x: 4, y: 8, z: 8, core: 2. Of those that a mesh axis runs over, the one named last changes fastest.
Arguments:
- mixed: bfloat16 [4096, 2048], P('sp'), may hold values from -6 to 6
- cotangent: bfloat16 [4096, 2048], P('sp'), may hold values from -6 to 6
- routes: int32 [4096, 2], P('sp'), may hold values from 0 to 31, all different within a row; in each aligned block of 128 rows (0 to 127, 128 to 255, ...) at most 16 rows name the same one
- gates: float32 [4096, 2], P('sp'), may hold values from 0.1 to 1
- w_gate: bfloat16 [32, 2048, 1024], P('sp', None, 'tp'), may hold values from -0.125 to 0.125
- w_up: bfloat16 [32, 2048, 1024], P('sp', None, 'tp'), may hold values from -0.125 to 0.125
- w_down: bfloat16 [32, 1024, 2048], P('sp', 'tp'), may hold values from -0.1875 to 0.1875
- out_weight: bfloat16 [4096, 2048], P('tp'), may hold values from -0.09375 to 0.09375
- gate_pre: bfloat16 [4096, 4096], P('sp', 'tp'), may hold values from -8 to 8
- mixer_out: bfloat16 [4096, 4096], P('sp', 'tp'), may hold values from -6 to 6
- values: bfloat16 [4096, 4096], P('sp', 'tp'), may hold values from -6 to 6
- write_keys: bfloat16 [4096, 2048], P('sp', 'tp'), may hold values from -1.25 to 1.25
- read_keys: bfloat16 [4096, 2048], P('sp', 'tp'), may hold values from -1.25 to 1.25
- log_decay: float32 [64, 4096], P('tp', 'sp'), may hold values from -0.08 to 0
- entry_states: float32 [32, 64, 64, 128], P('sp', 'tp'), may hold values from -6 to 6
Outputs:
- d_w_gate: bfloat16 [32, 2048, 1024], P('sp', None, 'tp')
- d_w_up: bfloat16 [32, 2048, 1024], P('sp', None, 'tp')
- d_w_down: bfloat16 [32, 1024, 2048], P('sp', 'tp')
- d_out_weight: float32 [2048, 4096], P('sp', 'tp')
- d_input: bfloat16 [4096, 2048], P('sp', 'tp')
- d_values: bfloat16 [4096, 4096], P('sp', 'tp')
- d_write: float32 [4096, 2048], P('sp', 'tp')
- d_read: float32 [4096, 2048], P('sp', 'tp')
- d_gate: bfloat16 [4096, 4096], P('sp', 'tp')
Inputs may be any that keep to these rules, and one draw needn't show every extreme that they name: `routes`: each row names 2 different experts; in the 128 rows of one device no expert is named more than 16 times, and in some blocks one is named exactly 16 times.
All inputs are finite; a program needn't handle non-finite values.
Results may differ from a plain program's by a relative error of at most 0.0062.
Values may be sent and summed in bfloat16 or wider, within the bound.
No kernel may reach another device: no remote copies, remote signals or barrier semaphores. Data moves between devices by JAX's collectives and lax.ppermute only.
A program may use at most 64 MiB of HBM per device.

v0:
```python
import jax
import jax.numpy as jnp
from jax import lax
from jax.sharding import Mesh
from jax.sharding import PartitionSpec as P

D = 2048
HEAD_DIM = 64
BLOCK = 128
TOPK = 2
TOK_DEV = 128
SP = ("sp_0", "sp_1")
precise = lax.Precision.HIGHEST


def sent_together(arrays, axis, split_dim, concat_dim, along):
    widths = [a.shape[along] for a in arrays]
    both = jnp.concatenate(arrays, axis=along)
    out = lax.all_to_all(both, axis, split_axis=split_dim, concat_axis=concat_dim, tiled=True)
    return tuple(jnp.split(out, [sum(widths[:k]) for k in range(1, len(widths))], axis=along))


def in_one_piece(arrays, axis, dim, along):
    widths = [a.shape[along] for a in arrays]
    both = jnp.concatenate(arrays, axis=along)
    out = lax.all_gather(both, axis, axis=dim, tiled=True)
    return tuple(jnp.split(out, [sum(widths[:k]) for k in range(1, len(widths))], axis=along))


def split_up(value, dim, count):
    before, after = (value.shape[:dim], value.shape[dim + 1 :])
    return jnp.moveaxis(value.reshape(*before, count, -1, *after), dim, 0)


def sent_and_summed(value, axis, dim):
    count = lax.axis_size(axis)
    parts = lax.all_to_all(split_up(value, dim, count), axis, 0, 0, tiled=True)
    return jnp.sum(parts, axis=0)


def filled_with(value, identity):
    return jax.tree.map(
        lambda a, e: jnp.broadcast_to(jnp.asarray(e, a.dtype), a.shape), value, identity
    )


def prefix_by_axis(value, axes, combine, identity):
    before = start = filled_with(value, identity)
    running = value
    for axis in reversed(axes):
        count, mine = (lax.axis_size(axis), lax.axis_index(axis))
        pieces = jax.tree.map(lambda part: lax.all_gather(part, axis), running)
        inside, running = (start, start)
        for k in reversed(range(count)):
            passed = k > mine
            running = combine(running, jax.tree.map(lambda part: part[k], pieces))
            inside = jax.tree.map(lambda new, old: jnp.where(passed, new, old), running, inside)
        before = combine(inside, before)
    return before


def silu_grad(pre_act):
    logistic = jax.nn.sigmoid(pre_act)
    return logistic * (1.0 + pre_act * (1.0 - logistic))


def contract_rows(first_op, second_op):
    return lax.dot_general(
        first_op, second_op, (((0,), (0,)), ((), ())), preferred_element_type=jnp.float32
    )


def contract_cols(first_op, second_op):
    return lax.dot_general(
        first_op, second_op, (((1,), (1,)), ((), ())), preferred_element_type=jnp.float32
    )


def combine_state(earlier, later):
    return (later[0] * earlier[0], later[1] + later[0][:, None, None] * earlier[1])


def block_back(grad_state, inputs_x, grad_y, log_rate, write_rows, read_rows, start_state):
    block_len = log_rate.shape[0]
    running = jnp.cumsum(log_rate, axis=0)
    causal_mask = (jnp.arange(block_len)[:, None] >= jnp.arange(block_len)[None, :])[:, :, None]
    spread = running[:, None, :] - running[None, :, :]
    decay_mat = jnp.where(causal_mask, jnp.exp(jnp.where(causal_mask, spread, 0.0)), 0.0)
    intersection = jnp.dot(read_rows, write_rows.T, precision=precise)
    mixing = intersection[:, :, None] * decay_mat
    to_end = jnp.exp(running[-1][None, :] - running)
    from_start = jnp.exp(running)
    grad_x = jnp.einsum("lsj,ljp->sjp", mixing, grad_y, precision=precise) + to_end[
        :, :, None
    ] * jnp.einsum("sn,jpn->sjp", write_rows, grad_state, precision=precise)
    weighted = jnp.einsum("ljp,sjp->lsj", grad_y, inputs_x, precision=precise) * decay_mat
    grad_w = jnp.einsum("lsj,ln->sn", weighted, read_rows, precision=precise) + jnp.einsum(
        "sj,sjp,jpn->sn", to_end, inputs_x, grad_state, precision=precise
    )
    grad_r = jnp.einsum("lsj,sn->ln", weighted, write_rows, precision=precise) + jnp.einsum(
        "lj,ljp,jpn->ln", from_start, grad_y, start_state, precision=precise
    )
    earlier = jnp.exp(running[-1])[:, None, None] * grad_state + jnp.einsum(
        "lj,ljp,ln->jpn", from_start, grad_y, read_rows, precision=precise
    )
    return (earlier, grad_x, grad_w, grad_r)


def body(
    mixed,
    cotangent,
    routes,
    gates,
    w_gate,
    w_up,
    w_down,
    out_weight,
    gate_pre,
    mixer_out,
    values,
    write_keys,
    read_keys,
    log_decay,
    entry_states,
):
    sp_count = lax.axis_size(SP)
    tp_count = lax.axis_size("tp")
    capacity = 4 * TOK_DEV // sp_count
    assigned = TOK_DEV * TOPK
    picks = routes.reshape(assigned)
    onehot = (picks[:, None] == jnp.arange(sp_count, dtype=jnp.int32)[None, :]).astype(jnp.int32)
    earlier_same = jnp.cumsum(onehot, axis=0) - onehot
    slot_of = jnp.sum(earlier_same * onehot, axis=1)
    target = picks * capacity + slot_of
    anchor = (
        jnp.full((sp_count * capacity,), assigned, jnp.int32)
        .at[target]
        .set(jnp.arange(assigned, dtype=jnp.int32))
    )
    weight_g = w_gate[0]
    weight_u = w_up[0]
    weight_d = w_down[0]
    column_count = D // tp_count
    offset = lax.axis_index("tp") * column_count
    tok_slice = lax.dynamic_slice_in_dim(mixed, offset, column_count, 1)
    cot_slice = lax.dynamic_slice_in_dim(cotangent, offset, column_count, 1)
    columns = tok_slice.shape[1]
    scaled = (
        (gates[:, :, None] * cot_slice[:, None, :].astype(jnp.float32))
        .astype(jnp.bfloat16)
        .reshape(assigned, columns)
    )
    empty_row = jnp.zeros((1, columns), jnp.bfloat16)
    cot_buffer = jnp.concatenate([scaled, empty_row])[anchor].reshape(sp_count, capacity, columns)
    tok_buffer = jnp.concatenate([tok_slice, empty_row])[anchor // TOPK].reshape(
        sp_count, capacity, columns
    )
    tok_buffer, cot_buffer = (tok_buffer, cot_buffer)
    tok_part, cot_part = sent_together((tok_buffer, cot_buffer), SP, 0, 0, 1)
    tok_rows, cot_rows = in_one_piece((tok_part, cot_part), "tp", 2, 0)
    expert_tok_rows = tok_rows
    expert_cot_rows = cot_rows
    expert_tok_rows = expert_tok_rows.reshape(-1, D)
    expert_cot_rows = expert_cot_rows.reshape(-1, D)
    pre_gate = jnp.dot(expert_tok_rows, weight_g, preferred_element_type=jnp.float32)
    pre_up = jnp.dot(expert_tok_rows, weight_u, preferred_element_type=jnp.float32)
    active = jax.nn.silu(pre_gate)
    hidden = (active * pre_up).astype(jnp.bfloat16)
    grad_down = contract_rows(hidden, expert_cot_rows)
    grad_hidden = contract_cols(expert_cot_rows, weight_d)
    grad_gate = (grad_hidden * pre_up * silu_grad(pre_gate)).astype(jnp.bfloat16)
    grad_upval = (grad_hidden * active).astype(jnp.bfloat16)
    grad_wg = contract_rows(expert_tok_rows, grad_gate)
    grad_wu = contract_rows(expert_tok_rows, grad_upval)
    partial_value = contract_cols(grad_gate, weight_g) + contract_cols(grad_upval, weight_u)
    grad_wg, grad_wu, grad_down, partial_value = (grad_wg, grad_wu, grad_down, partial_value)
    row_total = partial_value.shape[0]
    pieces = partial_value.astype(jnp.bfloat16).reshape(row_total, tp_count, column_count)
    received = lax.all_to_all(pieces, "tp", split_axis=1, concat_axis=1, tiled=True)
    summed = (
        jnp.sum(received.astype(jnp.float32), axis=1)
        .astype(jnp.bfloat16)
        .reshape(sp_count, capacity, column_count)
    )
    returned = lax.all_to_all(summed, SP, split_axis=0, concat_axis=0, tiled=True)
    columns = returned.shape[-1]
    picked = returned.reshape(sp_count * capacity, columns)[target].reshape(TOK_DEV, TOPK, columns)
    d_input = (cot_slice.astype(jnp.float32) + jnp.sum(picked.astype(jnp.float32), axis=1)).astype(
        jnp.bfloat16
    )
    whole = lax.all_gather(d_input, "tp", axis=1, tiled=True)
    back_proj = contract_cols(whole, out_weight)
    pre_act = gate_pre.astype(jnp.float32)
    gate_act = jax.nn.silu(pre_act)
    saved_out = mixer_out.astype(jnp.float32)
    d_gate = (back_proj * saved_out * silu_grad(pre_act)).astype(jnp.bfloat16)
    gated = (saved_out * gate_act).astype(jnp.bfloat16)
    d_out_weight = sent_and_summed(contract_rows(whole, gated), SP, 0)
    head_count = out_weight.shape[0] // HEAD_DIM
    grad_y = (back_proj * gate_act).reshape(TOK_DEV, head_count, HEAD_DIM)
    inputs_x = values.astype(jnp.float32).reshape(TOK_DEV, head_count, HEAD_DIM)
    write_rows = write_keys.astype(jnp.float32)
    read_rows = read_keys.astype(jnp.float32)
    log_rate = log_decay.T
    total_run = jnp.cumsum(log_rate, axis=0)
    shard_decay = jnp.exp(total_run[-1])
    shard_grad = jnp.einsum(
        "lj,ljp,ln->jpn", jnp.exp(total_run), grad_y, read_rows, precision=precise
    )
    identity = (jnp.ones_like(shard_decay), jnp.zeros_like(shard_grad))
    incoming = prefix_by_axis((shard_decay, shard_grad), SP, combine_state, identity)
    grad_state = incoming[1]
    pieces_x = []
    pieces_w = []
    pieces_r = []
    for block_id in reversed(range(TOK_DEV // BLOCK)):
        grad_state, grad_x, grad_w, grad_r = block_back(
            grad_state, inputs_x, grad_y, log_rate, write_rows, read_rows, entry_states[block_id]
        )
        pieces_x.insert(0, grad_x)
        pieces_w.insert(0, grad_w)
        pieces_r.insert(0, grad_r)
    d_values = pieces_x[0].reshape(TOK_DEV, head_count * HEAD_DIM).astype(jnp.bfloat16)
    d_write = pieces_w[0]
    d_read = pieces_r[0]
    return (
        grad_wg.astype(jnp.bfloat16)[None],
        grad_wu.astype(jnp.bfloat16)[None],
        grad_down.astype(jnp.bfloat16)[None],
        d_out_weight,
        d_input,
        d_values,
        d_write,
        d_read,
        d_gate,
    )


def solution(mesh):
    finer = Mesh(mesh.devices.reshape(8, 4, mesh.shape["tp"]), ("sp_0", "sp_1", "tp"))
    return jax.shard_map(
        body,
        mesh=finer,
        in_specs=(
            P(SP, None),
            P(SP, None),
            P(SP, None),
            P(SP, None),
            P(SP, None, "tp"),
            P(SP, None, "tp"),
            P(SP, "tp", None),
            P("tp", None),
            P(SP, "tp"),
            P(SP, "tp"),
            P(SP, "tp"),
            P(SP, "tp"),
            P(SP, "tp"),
            P("tp", SP),
            P(SP, "tp", None, None),
        ),
        out_specs=(
            P(SP, None, "tp"),
            P(SP, None, "tp"),
            P(SP, "tp", None),
            P(SP, "tp"),
            P(SP, "tp"),
            P(SP, "tp"),
            P(SP, "tp"),
            P(SP, "tp"),
            P(SP, "tp"),
        ),
        check_vma=False,
    )
```

profile of v0, /device:TPU:2, one launch (start us, length us, event | category | flops | bytes accessed | tf_op | source)
XLA Modules:
  0.0 289.5 jit_solution(18188501029784762102)
XLA Ops:
  11.2 1.4 scatter_custom_fusion
  13.6 1.3 gather_fusion.1
  15.0 1.3 gather_fusion
  16.4 24.5 %all_to_all.20 = bf16[32,32,128]{2,1,0:T(8,128)(2,1)S(1)} all-to-all(bf16[32,32,128]{2,1,0:T(8,128)(2,1)S(1)} %pad_maximum_fusion), channel_id=1, replica_groups=mesh['sp_0'=8,'sp_1'=4,'tp'=16] {'sp_0','sp_1'}, dimensions={0} | all-to-all | bytes 524288 | tf_op jit(solution)/shard_map/all_to_all | solution.py:19
  41.6 48.4 %all-gather.6.cloned.1.call-done = bf16[64,16,2048]{2,1,0:T(8,128)(2,1)} async-done(((bf16[64,16,128]{2,1,0:T(8,128)(2,1)}), bf16[64,16,2048]{2,1,0:T(8,128)(2,1)}) %all-gather.6.cloned.1.call-update) | async-done | bytes 4194320 | tf_op jit(solution)/shard_map/all_gather | solution.py:26
  90.1 2.6 fusion.77
  96.9 1.9 copy.65
  98.8 4.6 %all-to-all-start.1 = ((bf16[512,16,128]{2,0,1:T(8,128)(2,1)}), bf16[512,16,128]{2,0,1:T(8,128)(2,1)}, u32[]{:S(2)}, u32[]{:S(2)}) async-start(bf16[512,16,128]{2,0,1:T(8,128)(2,1)} %bitcast.231), calls=%async_computation.1 | async-start | bytes 4194304 | tf_op jit(solution)/shard_map/all_to_all | solution.py:179
  103.7 49.0 %all-to-all-done.1 = bf16[512,16,128]{2,0,1:T(8,128)(2,1)} async-done(((bf16[512,16,128]{2,0,1:T(8,128)(2,1)}), bf16[512,16,128]{2,0,1:T(8,128)(2,1)}, u32[]{:S(2)}, u32[]{:S(2)}) %all-to-all-start.1) | async-done | bytes 2097184 | tf_op jit(solution)/shard_map/all_to_all | solution.py:179
  152.6 2.6 reduce_sum.56
  155.2 10.5 %all-to-all-start.2 = ((bf16[32,16,128]{2,1,0:T(8,128)(2,1)}), bf16[32,16,128]{2,1,0:T(8,128)(2,1)S(1)}, u32[]{:S(2)}, u32[]{:S(2)}) async-start(bf16[32,16,128]{2,1,0:T(8,128)(2,1)} %bitcast.237), calls=%async_computation.2 | async-start | bytes 262144 | tf_op jit(solution)/shard_map/all_to_all | solution.py:185
  165.7 7.8 %all-gather.1 = f32[4,1,4]{2,1,0:T(1,128)S(1)} all-gather(f32[1,1,4]{2,1,0:T(1,128)S(1)} %get-tuple-element.47), channel_id=1, replica_groups=mesh['sp_0'=8,'sp_1'=4,'tp'=16] {'sp_1'}, dimensions={0}, use_global_device_ids=true | all-gather | bytes 80 | tf_op jit(solution)/shard_map/all_gather | solution.py:52
  174.8 0.9 gather_fusion.2
  176.6 16.8 %all_gather.25 = bf16[128,2048]{1,0:T(8,128)(2,1)S(1)} all-gather(bf16[128,128]{1,0:T(8,128)(2,1)S(1)} %add_convert_fusion.1), channel_id=1, replica_groups=mesh['sp_0'=8,'sp_1'=4,'tp'=16] {'tp'}, dimensions={1}, use_global_device_ids=true | all-gather | bytes 557056 | tf_op jit(solution)/shard_map/all_gather | solution.py:191
  194.3 2.7 fusion.56
  196.9 9.3 %all-to-all-start.3 = ((f32[32,64,256]{2,1,0:T(8,128)}), f32[32,64,256]{2,1,0:T(8,128)}, u32[]{:S(2)}, u32[]{:S(2)}) async-start(f32[32,64,256]{2,1,0:T(8,128)} %bitcast.230), calls=%async_computation.3 | async-start | bytes 4194304 | tf_op jit(solution)/shard_map/all_to_all | solution.py:37
  207.5 2.3 fusion.21
  209.7 1.0 copy.53
  210.9 18.1 %all-gather = f32[16,64,128]{2,1,0:T(8,128)S(1)} all-gather(f32[4,64,128]{2,1,0:T(8,128)S(1)} %fusion.54), channel_id=2, replica_groups=mesh['sp_0'=8,'sp_1'=4,'tp'=16] {'sp_1'}, dimensions={0}, use_global_device_ids=true | all-gather | bytes 655360 | tf_op jit(solution)/shard_map/all_gather | solution.py:52
  229.0 0.8 copy-done.3
  229.8 1.3 fusion.44
  231.9 0.9 copy.57
  232.8 1.6 copy.59
  234.4 31.3 %all-gather.2 = f32[8,1,4]{2,1,0:T(1,128)S(1)} all-gather(f32[1,1,4]{2,1,0:T(1,128)} %get-tuple-element.58), channel_id=1, replica_groups=mesh['sp_0'=8,'sp_1'=4,'tp'=16] {'sp_0'}, dimensions={0}, use_global_device_ids=true | all-gather | bytes 144 | tf_op jit(solution)/shard_map/all_gather | solution.py:52
  267.1 2.2 fusion.1
  269.3 1.2 fusion.2
  270.6 1.2 fusion
  272.7 0.8 convolution_add_fusion
  273.5 2.4 all-gather.8.cloned.1.call-done
  276.0 1.6 fusion.37
  279.5 0.9 convolution_add_fusion.1
  280.3 2.3 reduce_sum.58
  (139 shorter events, 19.4 us)
Async XLA Ops:
  7.2 200.3 %copy-start = (bf16[256,2048]{1,0:T(8,128)(2,1)S(1)}, bf16[256,2048]{1,0:T(8,128)(2,1)}, u32[]{:S(2)}) copy-start(bf16[256,2048]{1,0:T(8,128)(2,1)} %param.22) | copy-start | bytes 3145732
  7.2 82.9 %all-gather.6.cloned.1.call-start = ((), (), s32[]{:S(2)}) async-start(), calls=%async_computation.4 | async-start | bytes 4456448 | tf_op jit(solution)/shard_map/all_gather | solution.py:26
  41.6 51.1 %copy-start.6 = (bf16[1,2048,64]{1,2,0:T(8,128)(2,1)S(1)}, bf16[1,2048,64]{1,2,0:T(8,128)(2,1)}, u32[]{:S(2)}) copy-start(bf16[1,2048,64]{1,2,0:T(8,128)(2,1)} %param.19) | copy-start | bytes 786436
  98.8 4.6 %copy-start.37 = (f32[4,128]{1,0:T(4,128)S(1)}, f32[4,128]{1,0:T(4,128)}, u32[]{:S(2)}) copy-start(f32[4,128]{1,0:T(4,128)} %param.28) | copy-start | bytes 6148
  98.8 53.9 %all-to-all-start.1 = ((bf16[512,16,128]{2,0,1:T(8,128)(2,1)}), bf16[512,16,128]{2,0,1:T(8,128)(2,1)}, u32[]{:S(2)}, u32[]{:S(2)}) async-start(bf16[512,16,128]{2,0,1:T(8,128)(2,1)} %bitcast.231), calls=%async_computation.1 | async-start | bytes 4194304 | tf_op jit(solution)/shard_map/all_to_all | solution.py:179
  155.2 19.6 %all-to-all-start.2 = ((bf16[32,16,128]{2,1,0:T(8,128)(2,1)}), bf16[32,16,128]{2,1,0:T(8,128)(2,1)S(1)}, u32[]{:S(2)}, u32[]{:S(2)}) async-start(bf16[32,16,128]{2,1,0:T(8,128)(2,1)} %bitcast.237), calls=%async_computation.2 | async-start | bytes 262144 | tf_op jit(solution)/shard_map/all_to_all | solution.py:185
  176.6 20.3 %copy-start.21 = (bf16[128,128]{1,0:T(8,128)(2,1)}, bf16[128,128]{1,0:T(8,128)(2,1)S(1)}, u32[]{:S(2)}) copy-start(bf16[128,128]{1,0:T(8,128)(2,1)S(1)} %add_convert_fusion.1) | copy-start | bytes 98308
  196.9 9.9 %copy-start.17 = (f32[128,4]{1,0:T(8,128)S(1)}, f32[128,4]{1,0:T(8,128)}, u32[]{:S(2)}) copy-start(f32[128,4]{1,0:T(8,128)} %get-tuple-element.45) | copy-start | bytes 6148
  196.9 83.4 %all-to-all-start.3 = ((f32[32,64,256]{2,1,0:T(8,128)}), f32[32,64,256]{2,1,0:T(8,128)}, u32[]{:S(2)}, u32[]{:S(2)}) async-start(f32[32,64,256]{2,1,0:T(8,128)} %bitcast.230), calls=%async_computation.3 | async-start | bytes 4194304 | tf_op jit(solution)/shard_map/all_to_all | solution.py:37
  206.3 4.5 %copy-start.12 = (bf16[128,128]{1,0:T(8,128)(2,1)S(1)}, bf16[128,128]{1,0:T(8,128)(2,1)}, u32[]{:S(2)}) copy-start(bf16[128,128]{1,0:T(8,128)(2,1)} %param.27) | copy-start | bytes 98308
  206.3 69.6 %all-gather.8.cloned.1.call-start = ((), (), s32[]{:S(2)}) async-start(), calls=%async_computation.5 | async-start | bytes 1179648 | tf_op jit(solution)/shard_map/all_gather | solution.py:52
  207.4 22.4 %copy-start.25 = (f32[4]{0:T(128)S(1)}, f32[4]{0:T(128)}, u32[]{:S(2)}) copy-start(f32[4]{0:T(128)} %get-tuple-element.60) | copy-start | bytes 52
  207.5 58.9 %copy-start.10 = (bf16[128,128]{1,0:T(8,128)(2,1)S(1)}, bf16[128,128]{1,0:T(8,128)(2,1)}, u32[]{:S(2)}) copy-start(bf16[128,128]{1,0:T(8,128)(2,1)} %param.26) | copy-start | bytes 98308
  234.4 34.9 %copy-start.15 = (bf16[512,64]{0,1:T(8,128)(2,1)S(1)}, bf16[512,64]{0,1:T(8,128)(2,1)}, u32[]{:S(2)}) copy-start(bf16[512,64]{0,1:T(8,128)(2,1)} %copy-done.14) | copy-start | bytes 196612
  265.7 6.5 %copy-start.23 = (pred[128,128]{1,0:T(8,128)(4,1)}, pred[128,128]{1,0:T(8,128)(4,1)S(1)}, u32[]{:S(2)}) copy-start(pred[128,128]{1,0:T(8,128)(4,1)S(1)} %iota_compare_fusion) | copy-start | bytes 49156
  270.5 5.4 %copy-start.4 = (f32[16,64,128]{2,1,0:T(8,128)S(1)}, f32[16,64,128]{2,1,0:T(8,128)}, u32[]{:S(2)}) copy-start(f32[16,64,128]{2,1,0:T(8,128)} %copy-done.3) | copy-start | bytes 1572868
  270.5 5.4 %copy-start.26 = (f32[4]{0:T(128)S(1)}, f32[4]{0:T(128)}, u32[]{:S(2)}) copy-start(f32[4]{0:T(128)} %get-tuple-element.60) | copy-start | bytes 52
  270.5 5.4 %copy-start.27 = (f32[4]{0:T(128)S(1)}, f32[4]{0:T(128)}, u32[]{:S(2)}) copy-start(f32[4]{0:T(128)} %get-tuple-element.61) | copy-start | bytes 52
  270.5 5.4 %copy-start.28 = (f32[4]{0:T(128)S(1)}, f32[4]{0:T(128)}, u32[]{:S(2)}) copy-start(f32[4]{0:T(128)} %get-tuple-element.56) | copy-start | bytes 52
  270.5 5.4 %copy-start.29 = (f32[4]{0:T(128)S(1)}, f32[4]{0:T(128)}, u32[]{:S(2)}) copy-start(f32[4]{0:T(128)} %get-tuple-element.48) | copy-start | bytes 52
  270.5 5.4 %copy-start.30 = (f32[4]{0:T(128)S(1)}, f32[4]{0:T(128)}, u32[]{:S(2)}) copy-start(f32[4]{0:T(128)} %get-tuple-element.49) | copy-start | bytes 52
  270.5 5.4 %copy-start.31 = (f32[4]{0:T(128)S(1)}, f32[4]{0:T(128)}, u32[]{:S(2)}) copy-start(f32[4]{0:T(128)} %get-tuple-element.50) | copy-start | bytes 52
  270.5 5.4 %copy-start.32 = (f32[4]{0:T(128)S(1)}, f32[4]{0:T(128)}, u32[]{:S(2)}) copy-start(f32[4]{0:T(128)} %get-tuple-element.51) | copy-start | bytes 52
  270.6 5.4 %copy-start.33 = (f32[4]{0:T(128)S(1)}, f32[4]{0:T(128)}, u32[]{:S(2)}) copy-start(f32[4]{0:T(128)} %get-tuple-element.52) | copy-start | bytes 52
  270.6 5.4 %copy-start.34 = (f32[4]{0:T(128)S(1)}, f32[4]{0:T(128)}, u32[]{:S(2)}) copy-start(f32[4]{0:T(128)} %get-tuple-element.53) | copy-start | bytes 52
  270.6 5.4 %copy-start.35 = (f32[4]{0:T(128)S(1)}, f32[4]{0:T(128)}, u32[]{:S(2)}) copy-start(f32[4]{0:T(128)} %get-tuple-element.54) | copy-start | bytes 52
  270.6 5.4 %copy-start.36 = (f32[4]{0:T(128)S(1)}, f32[4]{0:T(128)}, u32[]{:S(2)}) copy-start(f32[4]{0:T(128)} %get-tuple-element.55) | copy-start | bytes 52
  271.8 6.0 %copy-start.22 = (f32[128,128]{1,0:T(8,128)S(1)}, f32[128,128]{1,0:T(8,128)}, u32[]{:S(2)}) copy-start(f32[128,128]{1,0:T(8,128)} %fusion.79) | copy-start | bytes 196612
  271.8 6.0 %copy-start.39 = (f32[128,4]{0,1:T(4,128)S(1)}, f32[128,4]{0,1:T(4,128)}, u32[]{:S(2)}) copy-start(f32[128,4]{0,1:T(4,128)} %copy.55) | copy-start | bytes 6148
  271.8 7.3 %copy-start.19 = (bf16[128,256]{0,1:T(8,128)(2,1)S(1)}, bf16[128,256]{0,1:T(8,128)(2,1)}, u32[]{:S(2)}) copy-start(bf16[128,256]{0,1:T(8,128)(2,1)} %copy.59) | copy-start | bytes 196612
  271.8 7.7 %copy-start.13 = (bf16[128,128]{1,0:T(8,128)(2,1)S(1)}, bf16[128,128]{1,0:T(8,128)(2,1)}, u32[]{:S(2)}) copy-start(bf16[128,128]{1,0:T(8,128)(2,1)} %param.27) | copy-start | bytes 98308
  272.7 5.2 %copy-start.24 = (pred[128,128]{1,0:T(8,128)(4,1)S(1)}, pred[128,128]{1,0:T(8,128)(4,1)}, u32[]{:S(2)}) copy-start(pred[128,128]{1,0:T(8,128)(4,1)} %copy-done.23) | copy-start | bytes 49156
  (14 other events, 27.0 us)
Sparse Core Ops, SparseCore 0:
  41.7 48.2 all-gather.5
  231.3 44.5 all-gather.7
where the time goes:
time: 290 us
  waiting for transfers between devices  100 us (34%)
  blocking collectives  98.5 us (34%)
  starting transfers between devices  24.5 us (8%)
  local copies, waits for them, and re-layouts  19.1 us (7%)
  matrix products  17.8 us (6%)
  between operations  14.7 us (5%)
  other arithmetic  14.5 us (5%)
    all_gather x3, blocking collectives, prefix_by_axis(): pieces = jax.tree.map(lambda part: lax.all_gather(part, axis), running)  57.2 us
    all_to_all x1, waiting for transfers between devices, body(): lax.all_to_all(pieces, 'tp', split_axis=1, concat_axis=1, tiled=True)  49 us
    all_gather x1, waiting for transfers between devices, in_one_piece(): out = lax.all_gather(both, axis, axis=dim, tiled=True)  48.4 us
    all_to_all x1, blocking collectives, sent_together(): lax.all_to_all(both, axis, split_axis=split_dim, concat_axis=concat_dim,...  24.5 us
    all_gather x1, blocking collectives, body(): whole = lax.all_gather(d_input, 'tp', axis=1, tiled=True)  16.8 us
    all_to_all x1, starting transfers between devices, body(): lax.all_to_all(summed, SP, split_axis=0, concat_axis=0, tiled=True)  10.5 us
    all_to_all x1, starting transfers between devices, sent_and_summed(): parts = lax.all_to_all(split_up(value, dim, count), axis, 0, 0, tiled=True)  9.32 us
    dot_general x4, matrix products, contract_rows(): lax.dot_general(first_op, second_op, (((0,), (0,)), ((), ())), preferred_...  7.21 us
  transfers between devices with their start and end apart: 5, of which 4 were waited for; matrix products, arithmetic and copies ran while one was open for 8% of the time, Pallas kernels for 0%

commit v1 on v0

--- a/solution.py
+++ b/solution.py
@@ -188,7 +188,13 @@
     d_input = (cot_slice.astype(jnp.float32) + jnp.sum(picked.astype(jnp.float32), axis=1)).astype(
         jnp.bfloat16
     )
-    whole = lax.all_gather(d_input, "tp", axis=1, tiled=True)
+    whole = lax.all_to_all(
+        jnp.concatenate([d_input for _ in range(lax.psum(1, "tp"))], axis=1),
+        axis_name="tp",
+        split_axis=1,
+        concat_axis=1,
+        tiled=True,
+    )
     back_proj = contract_cols(whole, out_weight)
     pre_act = gate_pre.astype(jnp.float32)
     gate_act = jax.nn.silu(pre_act)

time: 290 us -> 306 us (1.055)
  the two profiles are of different devices: /device:TPU:2 before, /device:TPU:4 now
where the time goes in v1:
time: 306 us; the launch traced here: 305 us
  blocking collectives  138 us (45%)
  waiting for transfers between devices  65.8 us (22%)
  local copies, waits for them, and re-layouts  32.7 us (11%)
  starting transfers between devices  21.3 us (7%)
  matrix products  17.9 us (6%)
  other arithmetic  15.1 us (5%)
  between operations  14.7 us (5%)
    all_gather x3, blocking collectives, prefix_by_axis(): pieces = jax.tree.map(lambda part: lax.all_gather(part, axis), running)  59.2 us
    all_to_all x1, blocking collectives, body(): lax.all_to_all(pieces, 'tp', split_axis=1, concat_axis=1, tiled=True)  53.9 us
    all_gather x1, waiting for transfers between devices, in_one_piece(): out = lax.all_gather(both, axis, axis=dim, tiled=True)  48.5 us
    all_to_all x1, blocking collectives, sent_together(): lax.all_to_all(both, axis, split_axis=split_dim, concat_axis=concat_dim,...  24.4 us
    unnamed x98, local copies, waits for them, and re-layouts  14 us
    all_to_all x1, starting transfers between devices, body(): lax.all_to_all(summed, SP, split_axis=0, concat_axis=0, tiled=True)  10.5 us
    all_to_all x1, waiting for transfers between devices, body(): lax.all_to_all(summed, SP, split_axis=0, concat_axis=0, tiled=True)  9.24 us
    dot_general x4, matrix products, contract_rows(): lax.dot_general(first_op, second_op, (((0,), (0,)), ((), ())), preferred_...  7.41 us
  transfers between devices with their start and end apart: 5, of which 4 were waited for; matrix products, arithmetic and copies ran while one was open for 7% of the time, Pallas kernels for 0%

profile of v1, /device:TPU:4, one launch (start us, length us, event | category | flops | bytes accessed | tf_op | source)
XLA Modules:
  0.0 305.2 jit_solution(14104793886351455867)
XLA Ops:
  11.2 1.4 scatter_custom_fusion
  13.6 1.3 gather_fusion.1
  15.0 1.3 gather_fusion
  16.4 24.4 %all_to_all.32 = bf16[32,32,128]{2,1,0:T(8,128)(2,1)S(1)} all-to-all(bf16[32,32,128]{2,1,0:T(8,128)(2,1)S(1)} %pad_maximum_fusion), channel_id=1, replica_groups=mesh['sp_0'=8,'sp_1'=4,'tp'=16] {'sp_0','sp_1'}, dimensions={0} | all-to-all | bytes 524288 | tf_op jit(solution)/shard_map/all_to_all | solution.py:19
  41.6 48.5 %all-gather.6.cloned.1.call-done = bf16[64,16,2048]{2,1,0:T(8,128)(2,1)} async-done(((bf16[64,16,128]{2,1,0:T(8,128)(2,1)}), bf16[64,16,2048]{2,1,0:T(8,128)(2,1)}) %all-gather.6.cloned.1.call-update) | async-done | bytes 4194320 | tf_op jit(solution)/shard_map/all_gather | solution.py:26
  90.0 2.8 fusion.78
  97.6 53.9 %all_to_all.33 = bf16[512,16,128]{2,0,1:T(8,128)(2,1)} all-to-all(bf16[512,16,128]{2,0,1:T(8,128)(2,1)S(1)} %bitcast.238), channel_id=1, replica_groups=mesh['sp_0'=8,'sp_1'=4,'tp'=16] {'tp'}, dimensions={1} | all-to-all | bytes 4194304 | tf_op jit(solution)/shard_map/all_to_all | solution.py:179
  151.5 2.6 reduce_sum.56
  154.1 10.5 %all-to-all-start.2 = ((bf16[32,16,128]{2,1,0:T(8,128)(2,1)}), bf16[32,16,128]{2,1,0:T(8,128)(2,1)S(1)}, u32[]{:S(2)}, u32[]{:S(2)}) async-start(bf16[32,16,128]{2,1,0:T(8,128)(2,1)} %bitcast.14), calls=%async_computation.2 | async-start | bytes 262144 | tf_op jit(solution)/shard_map/all_to_all | solution.py:185
  164.6 9.2 %all-to-all-done.2 = bf16[32,16,128]{2,1,0:T(8,128)(2,1)S(1)} async-done(((bf16[32,16,128]{2,1,0:T(8,128)(2,1)}), bf16[32,16,128]{2,1,0:T(8,128)(2,1)S(1)}, u32[]{:S(2)}, u32[]{:S(2)}) %all-to-all-start.2) | async-done | bytes 131104 | tf_op jit(solution)/shard_map/all_to_all | solution.py:185
  174.9 1.4 constant_dynamic-update-slice_fusion.15
  185.6 2.1 copy.88
  187.7 2.0 copy.89
  189.8 4.2 %all-to-all-start.3 = ((bf16[128,16,128]{2,0,1:T(8,128)(2,1)}), bf16[128,16,128]{2,0,1:T(8,128)(2,1)}, u32[]{:S(2)}, u32[]{:S(2)}) async-start(bf16[128,16,128]{2,0,1:T(8,128)(2,1)} %copy.89), calls=%async_computation.3 | async-start | bytes 1048576 | tf_op jit(solution)/shard_map/all_to_all | solution.py:191
  194.3 7.7 %all-gather.1 = f32[4,1,4]{2,1,0:T(1,128)S(1)} all-gather(f32[1,1,4]{2,1,0:T(1,128)S(1)} %get-tuple-element.67), channel_id=1, replica_groups=mesh['sp_0'=8,'sp_1'=4,'tp'=16] {'sp_1'}, dimensions={0}, use_global_device_ids=true | all-gather | bytes 80 | tf_op jit(solution)/shard_map/all_gather | solution.py:52
  202.6 7.3 %all-to-all-done.3 = bf16[128,16,128]{2,0,1:T(8,128)(2,1)} async-done(((bf16[128,16,128]{2,0,1:T(8,128)(2,1)}), bf16[128,16,128]{2,0,1:T(8,128)(2,1)}, u32[]{:S(2)}, u32[]{:S(2)}) %all-to-all-start.3) | async-done | bytes 524320 | tf_op jit(solution)/shard_map/all_to_all | solution.py:191
  209.9 2.1 copy.90
  212.0 2.9 fusion.57
  214.9 6.5 %all-to-all-start.4 = ((f32[32,64,256]{2,1,0:T(8,128)}), f32[32,64,256]{2,1,0:T(8,128)}, u32[]{:S(2)}, u32[]{:S(2)}) async-start(f32[32,64,256]{2,1,0:T(8,128)} %fusion.57), calls=%async_computation.4 | async-start | bytes 4194304 | tf_op jit(solution)/shard_map/all_to_all | solution.py:37
  222.6 2.2 fusion.21
  224.8 1.0 copy.91
  226.0 19.2 %all-gather = f32[16,64,128]{2,1,0:T(8,128)S(1)} all-gather(f32[4,64,128]{2,1,0:T(8,128)S(1)} %fusion.54), channel_id=2, replica_groups=mesh['sp_0'=8,'sp_1'=4,'tp'=16] {'sp_1'}, dimensions={0}, use_global_device_ids=true | all-gather | bytes 655360 | tf_op jit(solution)/shard_map/all_gather | solution.py:52
  246.1 1.3 fusion.44
  248.1 0.9 copy.95
  249.0 1.6 copy.97
  250.6 32.3 %all-gather.2 = f32[8,1,4]{2,1,0:T(1,128)S(1)} all-gather(f32[1,1,4]{2,1,0:T(1,128)} %get-tuple-element.78), channel_id=1, replica_groups=mesh['sp_0'=8,'sp_1'=4,'tp'=16] {'sp_0'}, dimensions={0}, use_global_device_ids=true | all-gather | bytes 144 | tf_op jit(solution)/shard_map/all_gather | solution.py:52
  284.3 2.2 fusion.1
  286.5 1.2 fusion.2
  287.8 1.2 fusion
  291.6 1.6 fusion.37
  295.1 0.9 convolution_add_fusion.1
  296.0 2.3 reduce_sum.58
  (155 shorter events, 30.4 us)
Async XLA Ops:
  7.2 215.4 %copy-start = (bf16[256,2048]{1,0:T(8,128)(2,1)S(1)}, bf16[256,2048]{1,0:T(8,128)(2,1)}, u32[]{:S(2)}) copy-start(bf16[256,2048]{1,0:T(8,128)(2,1)} %param.22) | copy-start | bytes 3145732
  7.2 82.9 %all-gather.6.cloned.1.call-start = ((), (), s32[]{:S(2)}) async-start(), calls=%async_computation.5 | async-start | bytes 4456448 | tf_op jit(solution)/shard_map/all_gather | solution.py:26
  41.6 51.3 %copy-start.6 = (bf16[1,2048,64]{1,2,0:T(8,128)(2,1)S(1)}, bf16[1,2048,64]{1,2,0:T(8,128)(2,1)}, u32[]{:S(2)}) copy-start(bf16[1,2048,64]{1,2,0:T(8,128)(2,1)} %param.19) | copy-start | bytes 786436
  154.1 19.8 %all-to-all-start.2 = ((bf16[32,16,128]{2,1,0:T(8,128)(2,1)}), bf16[32,16,128]{2,1,0:T(8,128)(2,1)S(1)}, u32[]{:S(2)}, u32[]{:S(2)}) async-start(bf16[32,16,128]{2,1,0:T(8,128)(2,1)} %bitcast.14), calls=%async_computation.2 | async-start | bytes 262144 | tf_op jit(solution)/shard_map/all_to_all | solution.py:185
  176.3 17.9 %copy-start.1 = (bf16[128,128]{1,0:T(8,128)(2,1)}, bf16[128,128]{1,0:T(8,128)(2,1)S(1)}, u32[]{:S(2)}) copy-start(bf16[128,128]{1,0:T(8,128)(2,1)S(1)} %get-tuple-element.55) | copy-start | bytes 98308
  176.3 17.7 %copy-start.36 = (f32[4,128]{1,0:T(4,128)S(1)}, f32[4,128]{1,0:T(4,128)}, u32[]{:S(2)}) copy-start(f32[4,128]{1,0:T(4,128)} %param.28) | copy-start | bytes 6148
  185.6 26.4 %copy-start.20 = (bf16[128,256]{1,0:T(8,128)(2,1)S(1)}, bf16[128,256]{1,0:T(8,128)(2,1)}, u32[]{:S(2)}) copy-start(bf16[128,256]{1,0:T(8,128)(2,1)} %param.24) | copy-start | bytes 196612
  189.8 20.2 %all-to-all-start.3 = ((bf16[128,16,128]{2,0,1:T(8,128)(2,1)}), bf16[128,16,128]{2,0,1:T(8,128)(2,1)}, u32[]{:S(2)}, u32[]{:S(2)}) async-start(bf16[128,16,128]{2,0,1:T(8,128)(2,1)} %copy.89), calls=%async_computation.3 | async-start | bytes 1048576 | tf_op jit(solution)/shard_map/all_to_all | solution.py:191
  214.9 81.1 %all-to-all-start.4 = ((f32[32,64,256]{2,1,0:T(8,128)}), f32[32,64,256]{2,1,0:T(8,128)}, u32[]{:S(2)}, u32[]{:S(2)}) async-start(f32[32,64,256]{2,1,0:T(8,128)} %fusion.57), calls=%async_computation.4 | async-start | bytes 4194304 | tf_op jit(solution)/shard_map/all_to_all | solution.py:37
  221.4 4.4 %copy-start.12 = (bf16[128,128]{1,0:T(8,128)(2,1)S(1)}, bf16[128,128]{1,0:T(8,128)(2,1)}, u32[]{:S(2)}) copy-start(bf16[128,128]{1,0:T(8,128)(2,1)} %param.27) | copy-start | bytes 98308
  221.4 70.1 %all-gather.8.cloned.1.call-start = ((), (), s32[]{:S(2)}) async-start(), calls=%async_computation.6 | async-start | bytes 1179648 | tf_op jit(solution)/shard_map/all_gather | solution.py:52
  222.0 25.5 %copy-start.24 = (f32[4]{0:T(128)}, f32[4]{0:T(128)S(1)}, u32[]{:S(2)}) copy-start(f32[4]{0:T(128)S(1)} %get-tuple-element.80) | copy-start | bytes 52
  222.6 61.0 %copy-start.10 = (bf16[128,128]{1,0:T(8,128)(2,1)S(1)}, bf16[128,128]{1,0:T(8,128)(2,1)}, u32[]{:S(2)}) copy-start(bf16[128,128]{1,0:T(8,128)(2,1)} %param.26) | copy-start | bytes 98308
  250.6 35.9 %copy-start.15 = (bf16[512,64]{0,1:T(8,128)(2,1)S(1)}, bf16[512,64]{0,1:T(8,128)(2,1)}, u32[]{:S(2)}) copy-start(bf16[512,64]{0,1:T(8,128)(2,1)} %copy-done.14) | copy-start | bytes 196612
  282.9 6.5 %copy-start.22 = (pred[128,128]{1,0:T(8,128)(4,1)}, pred[128,128]{1,0:T(8,128)(4,1)S(1)}, u32[]{:S(2)}) copy-start(pred[128,128]{1,0:T(8,128)(4,1)S(1)} %iota_compare_fusion) | copy-start | bytes 49156
  287.7 3.8 %copy-start.5 = (f32[16,64,128]{2,1,0:T(8,128)S(1)}, f32[16,64,128]{2,1,0:T(8,128)}, u32[]{:S(2)}) copy-start(f32[16,64,128]{2,1,0:T(8,128)} %copy-done.4) | copy-start | bytes 1572868
  287.7 3.8 %copy-start.25 = (f32[4]{0:T(128)S(1)}, f32[4]{0:T(128)}, u32[]{:S(2)}) copy-start(f32[4]{0:T(128)} %copy-done.24) | copy-start | bytes 52
  287.7 3.8 %copy-start.26 = (f32[4]{0:T(128)S(1)}, f32[4]{0:T(128)}, u32[]{:S(2)}) copy-start(f32[4]{0:T(128)} %get-tuple-element.81) | copy-start | bytes 52
  287.7 3.8 %copy-start.27 = (f32[4]{0:T(128)S(1)}, f32[4]{0:T(128)}, u32[]{:S(2)}) copy-start(f32[4]{0:T(128)} %get-tuple-element.76) | copy-start | bytes 52
  287.8 3.8 %copy-start.28 = (f32[4]{0:T(128)S(1)}, f32[4]{0:T(128)}, u32[]{:S(2)}) copy-start(f32[4]{0:T(128)} %get-tuple-element.68) | copy-start | bytes 52
  287.8 3.8 %copy-start.29 = (f32[4]{0:T(128)S(1)}, f32[4]{0:T(128)}, u32[]{:S(2)}) copy-start(f32[4]{0:T(128)} %get-tuple-element.69) | copy-start | bytes 52
  287.8 3.8 %copy-start.30 = (f32[4]{0:T(128)S(1)}, f32[4]{0:T(128)}, u32[]{:S(2)}) copy-start(f32[4]{0:T(128)} %get-tuple-element.70) | copy-start | bytes 52
  287.8 3.8 %copy-start.31 = (f32[4]{0:T(128)S(1)}, f32[4]{0:T(128)}, u32[]{:S(2)}) copy-start(f32[4]{0:T(128)} %get-tuple-element.71) | copy-start | bytes 52
  287.8 3.8 %copy-start.32 = (f32[4]{0:T(128)S(1)}, f32[4]{0:T(128)}, u32[]{:S(2)}) copy-start(f32[4]{0:T(128)} %get-tuple-element.72) | copy-start | bytes 52
  287.8 3.8 %copy-start.33 = (f32[4]{0:T(128)S(1)}, f32[4]{0:T(128)}, u32[]{:S(2)}) copy-start(f32[4]{0:T(128)} %get-tuple-element.73) | copy-start | bytes 52
  287.8 3.8 %copy-start.34 = (f32[4]{0:T(128)S(1)}, f32[4]{0:T(128)}, u32[]{:S(2)}) copy-start(f32[4]{0:T(128)} %get-tuple-element.74) | copy-start | bytes 52
  287.8 3.8 %copy-start.35 = (f32[4]{0:T(128)S(1)}, f32[4]{0:T(128)}, u32[]{:S(2)}) copy-start(f32[4]{0:T(128)} %get-tuple-element.75) | copy-start | bytes 52
  289.0 4.4 %copy-start.21 = (f32[128,128]{1,0:T(8,128)S(1)}, f32[128,128]{1,0:T(8,128)}, u32[]{:S(2)}) copy-start(f32[128,128]{1,0:T(8,128)} %fusion.80) | copy-start | bytes 196612
  289.0 4.4 %copy-start.38 = (f32[128,4]{0,1:T(4,128)S(1)}, f32[128,4]{0,1:T(4,128)}, u32[]{:S(2)}) copy-start(f32[128,4]{0,1:T(4,128)} %copy.93) | copy-start | bytes 6148
  289.0 5.7 %copy-start.18 = (bf16[128,256]{0,1:T(8,128)(2,1)S(1)}, bf16[128,256]{0,1:T(8,128)(2,1)}, u32[]{:S(2)}) copy-start(bf16[128,256]{0,1:T(8,128)(2,1)} %copy.97) | copy-start | bytes 196612
  289.0 6.1 %copy-start.13 = (bf16[128,128]{1,0:T(8,128)(2,1)S(1)}, bf16[128,128]{1,0:T(8,128)(2,1)}, u32[]{:S(2)}) copy-start(bf16[128,128]{1,0:T(8,128)(2,1)} %param.27) | copy-start | bytes 98308
  289.9 3.6 %copy-start.23 = (pred[128,128]{1,0:T(8,128)(4,1)S(1)}, pred[128,128]{1,0:T(8,128)(4,1)}, u32[]{:S(2)}) copy-start(pred[128,128]{1,0:T(8,128)(4,1)} %copy-done.22) | copy-start | bytes 49156
  (13 other events, 26.2 us)
Sparse Core Ops, SparseCore 0:
  41.7 48.2 all-gather.5
  247.6 43.9 all-gather.7
